TPU v7x, 32 devices: a whole 2x2x4 slice. The times are simulated.
32 devices in a mesh: sp: 16 (over z, y, x), tp: 2 (over core).
Axes of the slice: x: 2, y: 2, z: 4, core: 2. Of those that a mesh axis runs over, the one named last changes fastest.
Arguments:
- inputs: bfloat16 [4096, 2048], P('sp', 'tp'), may hold values from -200 to 200
- input_gain: bfloat16 [2048], P('tp'), may hold values from 0.099609375 to 1.8984375
- stick_query_w: bfloat16 [2048, 1024], P(None, 'tp'), may hold values from -0.3125 to 0.3125
- stick_key_w: bfloat16 [2048, 1024], P(None, 'tp'), may hold values from -0.125 to 0.125
- stick_value_w: bfloat16 [2048, 1024], P(None, 'tp'), may hold values from -0.125 to 0.125
- ret_query_w: bfloat16 [2048, 2048], P(None, 'tp'), may hold values from -0.125 to 0.125
- ret_key_w: bfloat16 [2048, 2048], P(None, 'tp'), may hold values from -0.125 to 0.125
- ret_value_w: bfloat16 [2048, 2048], P(None, 'tp'), may hold values from -0.125 to 0.125
- stick_offset: float32 [8], P('tp'), may hold values from -17 to -2
- ret_log_decay: float32 [8], P('tp'), may hold values from -0.04 to 0, as said below
- initial_state: float32 [8, 256, 256], P('tp', 'sp'), may hold values from -38.4 to 38.4
- stick_gain: float32 [1024], P('tp'), may hold values from 0.1 to 1.9
- ret_gain: float32 [2048], P('tp'), may hold values from 0.1 to 1.9
- stick_out_w: bfloat16 [1024, 2048], P('tp', 'sp'), may hold values from -0.125 to 0.125
- ret_out_w: bfloat16 [2048, 2048], P('tp', 'sp'), may hold values from -0.09375 to 0.09375
Outputs:
- layer_out: bfloat16 [4096, 2048], P(('sp', 'tp'))
Inputs may be any that keep to these rules, and one draw needn't show every extreme that they name: `ret_log_decay`: every entry is negative.
All inputs are finite; a program needn't handle non-finite values.
Results may differ from a plain program's by a relative error of at most 0.017.
Values may be sent and summed in bfloat16 or wider, within the bound.
A program may use at most 128 MiB of HBM per device.

v0:
```python
import jax
import jax.numpy as jnp
from jax import lax
from jax.sharding import PartitionSpec as P

D = 2048
STICK_HEADS = 8
STICK_DIM = 128


epsilon = 1e-06
rope_base = 10000.0


def entering_2(value, axis, join, neutral):
    count, mine = (lax.axis_size(axis), lax.axis_index(axis))
    pieces = jax.tree.map(lambda part: lax.all_gather(part, axis), value)
    running = jax.tree.map(
        lambda part, zero: jnp.full_like(part, 0) + jnp.asarray(zero, part.dtype), value, neutral
    )

    def hop(position, running):
        longer = join(running, jax.tree.map(lambda part: part[position], pieces))
        return jax.tree.map(lambda new, old: jnp.where(position < mine, new, old), longer, running)

    return lax.fori_loop(0, count - 1, hop, running)


def rotate(values, positions):
    half_width = values.shape[-1] // 2
    inverse = rope_base ** (-jnp.arange(half_width, dtype=jnp.float32) / half_width)
    angles = positions.astype(jnp.float32)[:, None] * inverse[None, :]
    cosine = jnp.cos(angles)[:, None, :]
    sine_table = jnp.sin(angles)[:, None, :]
    first_half = values[..., :half_width]
    second_half = values[..., half_width:]
    return jnp.concatenate(
        [
            first_half * cosine - second_half * sine_table,
            second_half * cosine + first_half * sine_table,
        ],
        axis=-1,
    )


def stick_block(partial_state, queries, key_rows, value_rows, offsets, query_pos, key_pos):
    running, before = partial_state
    score_scale = queries.shape[2] ** (-0.5)
    scores = (
        jnp.einsum("thd,shd->hts", queries, key_rows, preferred_element_type=jnp.float32)
        * score_scale
        + offsets[:, None, None]
    )
    allowed = ((key_pos[None, :] < query_pos[:, None]) & (key_pos[None, :] >= 0))[None]
    remain = jnp.where(allowed, jax.nn.log_sigmoid(-scores), 0.0)
    suffix = lax.cumsum(remain, axis=2, reverse=True) - remain + before[:, :, None]
    weights = jnp.where(allowed, jnp.exp(jax.nn.log_sigmoid(scores) + suffix), 0.0).astype(
        jnp.bfloat16
    )
    running = running + jnp.einsum(
        "hts,shd->thd", weights, value_rows, preferred_element_type=jnp.float32
    )
    return (running, before + jnp.sum(remain, axis=2))


def sweep_keys(keys_all, values_all, query_rows, positions, offsets, key_span):
    row_count, head_count, head_width = query_rows.shape
    span_offsets = jnp.arange(key_span, dtype=jnp.int32)
    needed = (positions[row_count - 1] + key_span) // key_span

    def visit(visit_index, partial_state):
        key_start = (needed - 1 - visit_index) * key_span
        key_rows = lax.dynamic_slice_in_dim(keys_all, key_start, key_span, 0).reshape(
            key_span, head_count, head_width
        )
        value_rows = lax.dynamic_slice_in_dim(values_all, key_start, key_span, 0).reshape(
            key_span, head_count, head_width
        )
        return stick_block(
            partial_state,
            query_rows,
            key_rows,
            value_rows,
            offsets,
            positions,
            key_start + span_offsets,
        )

    start_carry = (
        jnp.zeros((row_count, head_count, head_width), jnp.float32),
        jnp.zeros((head_count, row_count), jnp.float32),
    )
    final_state = lax.fori_loop(0, needed, visit, start_carry)
    return final_state[0]


def body(
    inputs,
    input_gain,
    stick_query_w,
    stick_key_w,
    stick_value_w,
    ret_query_w,
    ret_key_w,
    ret_value_w,
    stick_offset,
    ret_log_decay,
    initial_state,
    stick_gain,
    ret_gain,
    stick_out_w,
    ret_out_w,
):
    tok_rows = inputs.shape[0]
    matrices = (stick_query_w, stick_key_w, stick_value_w, ret_query_w, ret_key_w, ret_value_w)
    own_squares = jnp.sum(jnp.square(inputs.astype(jnp.float32)), axis=1)
    squares = lax.psum(own_squares, "tp")
    scaled = (
        lax.all_gather(inputs, "tp", axis=1, tiled=True).astype(jnp.float32)
        * lax.all_gather(input_gain[None, :], "tp", axis=1, tiled=True).astype(jnp.float32)
    ).astype(jnp.bfloat16)
    projected = tuple(
        (jnp.dot(scaled, matrix, preferred_element_type=jnp.float32) for matrix in matrices)
    )
    row_scale = lax.rsqrt(squares / D + epsilon)
    stick_query, stick_key, stick_value, ret_query, ret_key, ret_value = tuple(
        ((running * row_scale[:, None]).astype(jnp.bfloat16) for running in projected)
    )
    head_count = stick_offset.shape[0]
    head_width = stick_query.shape[1] // head_count
    first_pos = lax.axis_index("sp") * tok_rows
    query_pos = first_pos + jnp.arange(tok_rows, dtype=jnp.int32)
    queries = stick_query.reshape(tok_rows, head_count, head_width)
    key_span = 4 * tok_rows
    keys_all, values_all = (
        lax.all_gather(stick_key, "sp", axis=0, tiled=True),
        lax.all_gather(stick_value, "sp", axis=0, tiled=True),
    )
    stick_total = sweep_keys(keys_all, values_all, queries, query_pos, stick_offset, key_span)
    stick_local = jnp.sum(jnp.square(stick_total), axis=(1, 2))
    stick_squares = lax.psum(stick_local, "tp")
    stick_scale = lax.rsqrt(stick_squares / (STICK_HEADS * STICK_DIM) + epsilon)
    stick_normed = (
        stick_total.reshape(tok_rows, head_count * head_width) * stick_scale[:, None] * stick_gain
    ).astype(jnp.bfloat16)
    state_full = lax.all_gather(initial_state, "sp", axis=1, tiled=True)
    ret_heads = ret_log_decay.shape[0]
    ret_width = ret_query.shape[1] // ret_heads
    turned_query = rotate(
        ret_query.reshape(tok_rows, ret_heads, ret_width).astype(jnp.float32), query_pos
    )
    turned_key = rotate(
        ret_key.reshape(tok_rows, ret_heads, ret_width).astype(jnp.float32), query_pos
    ) * ret_width ** (-0.5)
    ret_values = ret_value.reshape(tok_rows, ret_heads, ret_width).astype(jnp.float32)
    local_pos = jnp.arange(tok_rows, dtype=jnp.float32)
    distance = local_pos[:, None] - local_pos[None, :]
    decay_mask = jnp.where(
        distance[None] >= 0.0,
        jnp.exp(ret_log_decay[:, None, None] * jnp.maximum(distance, 0.0)[None]),
        0.0,
    )
    highest = lax.Precision.HIGHEST
    scores = jnp.einsum("thd,shd->hts", turned_query, turned_key, precision=highest) * decay_mask
    inner_part = jnp.einsum("hts,she->the", scores, ret_values, precision=highest)
    key_decay = jnp.exp(ret_log_decay[None, :] * (tok_rows - 1.0 - local_pos[:, None]))
    own_state = jnp.einsum(
        "shd,she->hde", turned_key * key_decay[:, :, None], ret_values, precision=highest
    )
    block_decay = jnp.exp(ret_log_decay * tok_rows)

    def join_states(earlier, later):
        return (earlier[0] * later[1][:, None, None] + later[0], earlier[1] * later[1])

    prefix_state, _ = entering_2(
        (own_state, block_decay),
        "sp",
        join_states,
        (jnp.zeros_like(own_state), jnp.ones_like(block_decay)),
    )
    entering = (
        prefix_state
        + jnp.exp(ret_log_decay * first_pos.astype(jnp.float32))[:, None, None] * state_full
    )
    query_decay = jnp.exp(ret_log_decay[None, :] * (local_pos[:, None] + 1.0))
    cross_part = (
        jnp.einsum("thd,hde->the", turned_query, entering, precision=highest)
        * query_decay[:, :, None]
    )
    ret_total = inner_part + cross_part
    centered = ret_total - jnp.mean(ret_total, axis=2, keepdims=True)
    normed = centered * lax.rsqrt(jnp.mean(centered * centered, axis=2, keepdims=True) + epsilon)
    ret_normed = (normed.reshape(tok_rows, ret_heads * ret_width) * ret_gain).astype(jnp.bfloat16)
    stick_cols, ret_cols = (
        lax.all_gather(stick_out_w, "sp", axis=1, tiled=True),
        lax.all_gather(ret_out_w, "sp", axis=1, tiled=True),
    )
    stick_part = jnp.dot(stick_normed, stick_cols, preferred_element_type=jnp.float32)
    return lax.psum_scatter(
        (stick_part + jnp.dot(ret_normed, ret_cols, preferred_element_type=jnp.float32)).astype(
            jnp.bfloat16
        ),
        "tp",
        scatter_dimension=0,
        tiled=True,
    )


def solution(mesh):
    in_specs = (
        P("sp", "tp"),
        P("tp"),
        P(None, "tp"),
        P(None, "tp"),
        P(None, "tp"),
        P(None, "tp"),
        P(None, "tp"),
        P(None, "tp"),
        P("tp"),
        P("tp"),
        P("tp", "sp", None),
        P("tp"),
        P("tp"),
        P("tp", "sp"),
        P("tp", "sp"),
    )
    out_specs = P(("sp", "tp"), None)
    return jax.shard_map(body, mesh=mesh, in_specs=in_specs, out_specs=out_specs, check_vma=False)
```

profile of v0, /device:TPU:0, one launch (start us, length us, event | category | flops | bytes accessed | tf_op | source)
XLA Modules:
  0.0 597.4 jit_solution(9106212903124527146)
XLA Ops:
  13.1 7.5 %all-gather.11.cloned.1.call-done = bf16[256,2048]{1,0:T(8,128)(2,1)} async-done(((bf16[256,1024]{1,0:T(8,128)(2,1)}), bf16[256,2048]{1,0:T(8,128)(2,1)}) %all-gather.11.cloned.1.call-update) | async-done | bytes 1048592 | tf_op jit(solution)/shard_map/all_gather | solution.py:119
  23.5 3.0 fusion.30
  27.3 3.4 fusion.26
  31.2 4.0 fusion.28
  46.4 43.1 %all-reduce = f32[64]{0:T(128)S(1)} all-reduce(f32[64]{0:T(128)S(1)} %get-tuple-element.346), channel_id=3, replica_groups=mesh['sp'=16,'tp'=2] {'sp'}, use_global_device_ids=true, to_apply=%add | all-reduce | flops 64 | bytes 512
  94.2 6.5 %all-gather.13.cloned.1.call-done = bf16[4096,512]{1,0:T(8,128)(2,1)} async-done(((bf16[256,512]{1,0:T(8,128)(2,1)}), bf16[4096,512]{1,0:T(8,128)(2,1)}) %all-gather.13.cloned.1.call-update) | async-done | bytes 4194320 | tf_op jit(solution)/shard_map/all_gather | solution.py:137
  100.7 77.1 %all-gather.15.cloned.1.call-done = bf16[4096,512]{1,0:T(8,128)(2,1)} async-done(((bf16[256,512]{1,0:T(8,128)(2,1)}), bf16[4096,512]{1,0:T(8,128)(2,1)}) %all-gather.15.cloned.1.call-update) | async-done | bytes 4194320 | tf_op jit(solution)/shard_map/all_gather | solution.py:136
  178.7 34.5 %while.29 = (s32[]{:T(128)}, f32[256,4,128]{0,2,1:T(8,128)}, f32[4,256]{1,0:T(4,128)S(1)}, s32[]{:T(128)}, s32[]{:T(128)}, /*index=5*/bf16[4096,512]{1,0:T(8,128...) while((s32[]{:T(128)}, f32[256,4,128]{0,2,1:T(8,128)}, ...), condition=%wide.region_6.7_spmd.clone, body=%wide.region_2.6_spmd.clone.sunk | while | flops 707463424 | bytes 96735608 | solution.py:93
  181.8 6.3 %fusion.89 = (f32[4,256]{1,0:T(4,128)S(1)}, f32[4,256,1024]{1,2,0:T(8,128)S(1)}, f32[4,1024,256]{2,1,0:T(8,128)}) fusion(f32[4]{0:T(128)S(1)} %get-tuple-element.519, pred[256,1024]{0,1:T(8,128)(4,1)S(1)} %compare_and_fusion.2, bf16[1024,4,128]{0,2,1:T(8,128)(2,1)S(1)} %bitcast.121, bf16[256,4,128]{2,0,1:T(8,128)(2,1)} %get-tuple-element.518), kind=kOutput, calls=%fused_computation.33.clone.1 | convolution fusion | flops 279968768 | bytes 9965584 | tf_op jit(solution)/shard_map/while/body/thd,shd->hts/dot_general | solution.py:50
  188.1 10.1 %fusion.90 = f32[4,256,8,128]{1,2,3,0:T(8,128)S(1)} fusion(f32[4,256,8,128]{1,3,2,0:T(8,128)S(1)} %bitcast.119), kind=kOutput, calls=%fused_computation.20.clone.1 | output fusion | flops 133169152 | bytes 8388608 | tf_op jit(solution)/shard_map/reduce-window.4
  205.2 6.6 %fusion.91 = bf16[4,256,1024]{1,2,0:T(8,128)(2,1)S(1)} fusion(f32[4,256,8,128]{1,3,2,0:T(8,128)S(1)} %copy.98, f32[4,1024,256]{2,1,0:T(8,128)S(1)} %copy-done.3, f32[4,256]{1,0:T(4,128)S(1)} %get-tuple-element.498, f32[4]{0:T(128)S(1)} %get-tuple-element.519, pred[256,1024]{0,1:T(8,128)(4,1)S(1)} %compare_and_fusion.2), kind=kLoop, calls=%fused_computation.8.clone.1 | loop fusion | flops 24117248 | bytes 10752016 | tf_op jit(solution)/shard_map/while/body/convert_element_type | solution.py:57
  218.2 151.9 %all-gather.23.cloned.1.call-done = f32[64,256,256]{2,1,0:T(8,128)} async-done(((f32[4,256,256]{2,1,0:T(8,128)}), f32[64,256,256]{2,1,0:T(8,128)}) %all-gather.23.cloned.1.call-update) | async-done | bytes 16777232 | tf_op jit(solution)/shard_map/all_gather | solution.py:17
  370.1 41.3 %while.30 = (s32[]{:T(128)}, f32[4,256,256]{2,1,0:T(8,128)}, s32[]{:T(128)}, f32[16,4]{1,0:T(8,128)S(1)}, f32[16,4,256,256]{3,2,1,0:T(8,128)}, /*index=5*/s32[]{:T(128)}, s32[]{:T(128)}) while((s32[]{:T(128)}, f32[4,256,256]{2,1,0:T(8,128)}, s32[]{:T(128)}, f32[16,4]{1,0:T(8,128)S(1)}, f32[16,4,256,256]{3,2,1,0:T(8,128)}, ...), condition=%wide.region_10.11_spmd.clone, body=%wide.region_9.10_spmd.clone.sunk | while | flops 1048580 | bytes 3145889 | solution.py:26
  372.7 2.7 fusion.93
  375.4 2.7 fusion.93
  378.2 2.8 fusion.93
  381.0 2.7 fusion.93
  383.7 2.8 fusion.93
  386.5 2.7 fusion.93
  389.2 2.7 fusion.93
  392.0 2.7 fusion.93
  394.7 2.8 fusion.93
  397.6 2.7 fusion.93
  403.1 2.8 fusion.93
  408.6 2.7 fusion.93
  411.3 14.5 %all-gather.19.cloned.1.call-done = f32[4,256,256]{2,1,0:T(8,128)} async-done(((f32[4,16,256]{2,1,0:T(8,128)}), f32[4,256,256]{2,1,0:T(8,128)}) %all-gather.19.cloned.1.call-update) | async-done | bytes 1048592 | tf_op jit(solution)/shard_map/all_gather | solution.py:146
  425.8 3.5 fusion.57
  429.8 86.2 %all-gather.21.cloned.1.call-done = bf16[1024,2048]{1,0:T(8,128)(2,1)} async-done(((bf16[1024,128]{1,0:T(8,128)(2,1)}), bf16[1024,2048]{1,0:T(8,128)(2,1)}) %all-gather.21.cloned.1.call-update) | async-done | bytes 4194320 | tf_op jit(solution)/shard_map/all_gather | solution.py:196
  516.0 4.9 fusion.58
  520.9 58.9 %all-gather.17.cloned.1.call-done = bf16[512,2048]{1,0:T(8,128)(2,1)} async-done(((bf16[512,128]{1,0:T(8,128)(2,1)}), bf16[512,2048]{1,0:T(8,128)(2,1)}) %all-gather.17.cloned.1.call-update) | async-done | bytes 2097168 | tf_op jit(solution)/shard_map/all_gather | solution.py:195
  579.8 3.9 fusion.21
  583.8 6.7 %reduce-scatter.2.cloned.1.call-done = bf16[128,2048]{1,0:T(8,128)(2,1)} async-done(((bf16[256,2048]{1,0:T(8,128)(2,1)}), bf16[128,2048]{1,0:T(8,128)(2,1)}) %reduce-scatter.2.cloned.1.call-update) | async-done | bytes 524304 | tf_op jit(solution)/shard_map/reduce_scatter | solution.py:199
  (130 shorter events, 51.0 us)
Async XLA Ops:
  6.5 14.1 %copy-start = (bf16[2048,512]{1,0:T(8,128)(2,1)S(1)}, bf16[2048,512]{1,0:T(8,128)(2,1)}, u32[]{:S(2)}) copy-start(bf16[2048,512]{1,0:T(8,128)(2,1)} %param.23) | copy-start | bytes 6291460
  6.5 14.1 %all-gather.11.cloned.1.call-start = ((), (), s32[]{:S(2)}) async-start(), calls=%async_computation.1 | async-start | bytes 1572864 | tf_op jit(solution)/shard_map/all_gather | solution.py:119
  7.3 93.4 %all-gather.13.cloned.1.call-start = ((), (), s32[]{:S(2)}) async-start(), calls=%async_computation.2 | async-start | bytes 4456448 | tf_op jit(solution)/shard_map/all_gather | solution.py:137
  13.1 13.5 %copy-start.14 = (f32[4]{0:T(128)S(1)}, f32[4]{0:T(128)}, u32[]{:S(2)}) copy-start(f32[4]{0:T(128)} %param.28) | copy-start | bytes 52
  20.7 2.8 copy-start.17
  23.4 154.4 %all-gather.15.cloned.1.call-start = ((), (), s32[]{:S(2)}) async-start(), calls=%async_computation.3 | async-start | bytes 4456448 | tf_op jit(solution)/shard_map/all_gather | solution.py:136
  26.5 343.5 %all-gather.23.cloned.1.call-start = ((), (), s32[]{:S(2)}) async-start(), calls=%async_computation.8 | async-start | bytes 17825792 | tf_op jit(solution)/shard_map/all_gather | solution.py:17
  35.7 2.2 copy-start.15
  35.7 2.5 copy-start.18
  38.2 51.4 %copy-start.7 = (f32[256,4,128]{2,0,1:T(8,128)}, f32[256,4,128]{2,0,1:T(8,128)S(1)}, u32[]{:S(2)}) copy-start(f32[256,4,128]{2,0,1:T(8,128)S(1)} %get-tuple-element.333) | copy-start | bytes 1572868
  38.2 51.4 %copy-start.9 = (f32[256,4,128]{2,0,1:T(8,128)}, f32[256,4,128]{2,0,1:T(8,128)S(1)}, u32[]{:S(2)}) copy-start(f32[256,4,128]{2,0,1:T(8,128)S(1)} %get-tuple-element.334) | copy-start | bytes 1572868
  38.2 6.9 %copy-start.20 = (u32[32]{0:T(128)S(1)}, u32[32]{0:T(128)}, u32[]{:S(2)}) copy-start(u32[32]{0:T(128)} %constant.118) | copy-start | bytes 388
  41.7 384.1 %all-gather.19.cloned.1.call-start = ((), (), s32[]{:S(2)}) async-start(), calls=%async_computation.5 | async-start | bytes 1114112 | tf_op jit(solution)/shard_map/all_gather | solution.py:146
  42.2 473.7 %all-gather.21.cloned.1.call-start = ((), (), s32[]{:S(2)}) async-start(), calls=%async_computation.6 | async-start | bytes 4456448 | tf_op jit(solution)/shard_map/all_gather | solution.py:196
  42.8 537.0 %all-gather.17.cloned.1.call-start = ((), (), s32[]{:S(2)}) async-start(), calls=%async_computation.4 | async-start | bytes 2228224 | tf_op jit(solution)/shard_map/all_gather | solution.py:195
  43.6 547.0 %reduce-scatter.2.cloned.1.call-start = ((), (), s32[]{:S(2)}) async-start(), calls=%async_computation.7 | async-start | bytes 1572864 | tf_op jit(solution)/shard_map/reduce_scatter | solution.py:199
  89.5 3.2 copy-start.16
  89.5 3.2 copy-start.19
  90.9 87.8 %copy-start.11 = (f32[4]{0:T(128)S(1)}, f32[4]{0:T(128)}, u32[]{:S(2)}) copy-start(f32[4]{0:T(128)} %param.27) | copy-start | bytes 52
  178.7 38.3 %copy-start.13 = (f32[512]{0:T(512)S(1)}, f32[512]{0:T(512)}, u32[]{:S(2)}) copy-start(f32[512]{0:T(512)} %param.30) | copy-start | bytes 6148
  198.2 2.1 copy-start.2
  203.0 2.2 copy-start.3
  205.2 6.6 %copy-start.4 = (f32[256,4,128]{0,2,1:T(8,128)S(1)}, f32[256,4,128]{0,2,1:T(8,128)}, u32[]{:S(2)}) copy-start(f32[256,4,128]{0,2,1:T(8,128)} %get-tuple-element.497) | copy-start | bytes 1572868 | tf_op jit(solution)/shard_map/while
  212.3 0.8 copy-start.5
  370.1 55.7 %copy-start.6 = (f32[256,4,256]{0,2,1:T(8,128)S(1)}, f32[256,4,256]{0,2,1:T(8,128)}, u32[]{:S(2)}) copy-start(f32[256,4,256]{0,2,1:T(8,128)} %convolution_bitcast_fusion.2) | copy-start | bytes 3145732
  370.1 55.7 %copy-start.8 = (f32[256,4,128]{2,0,1:T(8,128)S(1)}, f32[256,4,128]{2,0,1:T(8,128)}, u32[]{:S(2)}) copy-start(f32[256,4,128]{2,0,1:T(8,128)} %copy-done.7) | copy-start | bytes 1572868
  370.1 55.7 %copy-start.10 = (f32[256,4,128]{2,0,1:T(8,128)S(1)}, f32[256,4,128]{2,0,1:T(8,128)}, u32[]{:S(2)}) copy-start(f32[256,4,128]{2,0,1:T(8,128)} %copy-done.9) | copy-start | bytes 1572868
  425.8 3.8 copy-start.12
  516.0 74.6 %copy-start.1 = (bf16[2048,512]{1,0:T(8,128)(2,1)S(1)}, bf16[2048,512]{1,0:T(8,128)(2,1)}, u32[]{:S(2)}) copy-start(bf16[2048,512]{1,0:T(8,128)(2,1)} %param.23) | copy-start | bytes 6291460
Sparse Core Ops, SparseCore 0:
  8.9 11.7 all-gather.10
  23.5 77.1 all-gather.12
  103.5 74.2 all-gather.14
  180.4 189.5 all-gather.22
  372.7 53.0 all-gather.18
  428.3 87.5 all-gather.20
  518.7 61.1 all-gather.16
  583.9 6.5 reduce-scatter.1
where the time goes:
time: 599 us; the launch traced here: 597 us
  waiting for transfers between devices  412 us (69%)
  other arithmetic  66 us (11%)
  blocking collectives  50.3 us (8%)
  matrix products  39.7 us (7%)
  between operations  15 us (3%)
  local copies, waits for them, and re-layouts  14 us (2%)
    all_gather x1, waiting for transfers between devices, entering_2(): pieces = jax.tree.map(lambda part: lax.all_gather(part, axis), value)  152 us
    all_gather x1, waiting for transfers between devices, body(): lax.all_gather(ret_out_w, 'sp', axis=1, tiled=True)  86.2 us
    all_gather x1, waiting for transfers between devices, body(): lax.all_gather(stick_key, 'sp', axis=0, tiled=True)  77.1 us
    all_gather x1, waiting for transfers between devices, body(): lax.all_gather(stick_out_w, 'sp', axis=1, tiled=True)  58.9 us
    unnamed x1, blocking collectives  43.1 us
    select_n x15, other arithmetic, hop(): jnp.where(position < mine, new, old)  41.1 us
    dot_general x6, matrix products, body(): jnp.dot(scaled, matrix, preferred_element_type=jnp.float32)  15.1 us
    all_gather x1, waiting for transfers between devices, body(): state_full = lax.all_gather(initial_state, 'sp', axis=1, tiled=True)  14.5 us
  transfers between devices with their start and end apart: 8, of which 8 were waited for; matrix products, arithmetic and copies ran while one was open for 18% of the time, Pallas kernels for 0%

commit v1 on v0

v1 whole, which is shorter than its diff:
```python
import functools
import math

import jax
import jax.numpy as jnp
from jax import lax
from jax.experimental import pallas as pl
from jax.experimental.pallas import tpu as pltpu
from jax.sharding import PartitionSpec as P

D = 2048
STICK_HEADS = 8
STICK_DIM = 128

epsilon = 1e-06
rope_base = 10000.0
MESH = pl.DeviceIdType.MESH
LOG2E = math.log2(math.e)


def mixer_kernel(
    n, heads,
    off_ref, q_ref, k_ref, v_ref, st_ref, init_ref, dec_ref,
    out_ref, ent_ref,
    kbuf, vbuf, qbuf, res, back, sbuf, ebuf, ent,
    k_send, v_send, q_send, r_send, s_send, e_send,
    k_recv, v_recv, q_recv, r_recv, s_recv, e_recv,
):
    me = lax.axis_index("sp")
    group = n // heads
    rows = q_ref.shape[0]
    width = q_ref.shape[1] // heads
    my_head = me // group
    my_slot = lax.rem(me, group)

    def flip(run, place):
        return jnp.where(lax.rem(run, 2) == 0, place, group - 1 - place)

    def columns(head):
        return pl.ds(pl.multiple_of(head * width, width), width)

    def copy(source, target, send, recv, peer):
        return pltpu.make_async_remote_copy(
            src_ref=source, dst_ref=target, send_sem=send, recv_sem=recv,
            device_id={"sp": peer}, device_id_type=MESH,
        )

    def arrived(target, recv):
        copy(target, target, recv, recv, me).wait_recv()

    def sent(source, send):
        copy(source, source, send, send, me).wait_send()

    barrier = pltpu.get_barrier_semaphore()
    for step in range(1, n):
        pl.semaphore_signal(
            barrier, inc=1, device_id={"sp": lax.rem(me + step, n)}, device_id_type=MESH
        )
    pl.semaphore_wait(barrier, n - 1)

    for step in range(1, n):
        peer = lax.rem(me + step, n)
        copy(st_ref.at[peer], sbuf.at[me], s_send.at[peer], s_recv.at[me], peer).start()
    my_run = me // group
    owner_slot = flip(my_run, my_slot)
    for head in range(heads):
        owner = head * group + owner_slot
        part = q_ref.at[:, head * width:(head + 1) * width]

        @pl.when(owner != me)
        def _():
            copy(part, qbuf.at[my_run], q_send.at[head], q_recv.at[my_run], owner).start()

        @pl.when(owner == me)
        def _():
            qbuf[my_run] = part[...]

    for step in range(1, n):
        peer = lax.rem(me + step, n)
        cols = columns(peer // group)
        copy(k_ref.at[:, cols], kbuf.at[me], k_send.at[peer], k_recv.at[me], peer).start()
        copy(v_ref.at[:, cols], vbuf.at[me], v_send.at[peer], v_recv.at[me], peer).start()
    kbuf[me] = k_ref[:, columns(my_head)]
    vbuf[me] = v_ref[:, columns(my_head)]
    sbuf[me] = st_ref[me]

    for source in range(n):
        @pl.when(source != me)
        def _():
            arrived(sbuf.at[source], s_recv.at[source])

    decay = dec_ref[...]
    state = init_ref[...]
    for place in range(n):
        ebuf[place] = state.astype(ebuf.dtype)
        if place < n - 1:
            state = state * decay + sbuf[place].astype(jnp.float32)
    for step in range(1, n):
        peer = lax.rem(me + step, n)
        copy(ebuf.at[peer], ent.at[me], e_send.at[peer], e_recv.at[me], peer).start()
    ent[me] = ebuf[me]

    offset = off_ref[my_head] * LOG2E
    factor = width ** (-0.5) * LOG2E
    row_at = lax.broadcasted_iota(jnp.int32, (rows, rows), 0)
    col_at = lax.broadcasted_iota(jnp.int32, (rows, rows), 1)
    below = col_at < row_at
    later = jnp.where(below, 1.0, 0.0).astype(jnp.bfloat16)

    def tile(query, keys, shift, mask):
        score = (
            lax.dot_general(
                query, keys, (((1,), (1,)), ((), ())), preferred_element_type=jnp.float32
            ) * factor + shift
        )
        soft = jnp.maximum(score, 0.0) + jnp.log(1.0 + jnp.exp2(-jnp.abs(score))) * LOG2E
        take = score - soft
        if mask is not None:
            soft = jnp.where(mask, soft, 0.0)
        suffix = jnp.dot(soft.astype(jnp.bfloat16), later, preferred_element_type=jnp.float32)
        return take - suffix, suffix[:, 0:1] + soft[:, 0:1]

    def weigh(power, mask, values):
        weight = jnp.exp2(power)
        if mask is not None:
            weight = jnp.where(mask, weight, 0.0)
        return jnp.dot(weight.astype(jnp.bfloat16), values, preferred_element_type=jnp.float32)

    for run in range(heads):
        block = run * group + flip(run, my_slot)
        for source in range(run * group, (run + 1) * group):
            @pl.when(source != me)
            def _():
                arrived(kbuf.at[source], k_recv.at[source])
                arrived(vbuf.at[source], v_recv.at[source])

        @pl.when(block != me)
        def _():
            arrived(qbuf.at[run], q_recv.at[run])

        query = qbuf[run]
        power, before = tile(query, kbuf[block], offset, below)
        total = weigh(power, below, vbuf[block])

        def visit(index, carry):
            total, before = carry
            first = block - 1 - 2 * index
            second = jnp.maximum(first - 1, 0)
            shift = jnp.where(first >= 1, offset, -1e9)
            power_a, gone_a = tile(query, kbuf[first], offset, None)
            power_b, gone_b = tile(query, kbuf[second], shift, None)
            middle = before + gone_a
            total = total + weigh(power_a - before, None, vbuf[first])
            total = total + weigh(power_b - middle, None, vbuf[second])
            return total, middle + gone_b

        total, _unused = lax.fori_loop(0, (block + 1) // 2, visit, (total, before))
        res[run] = total.astype(res.dtype)

        @pl.when(block != me)
        def _():
            copy(res.at[run], back.at[my_head], r_send.at[run], r_recv.at[my_head], block).start()

        @pl.when(block == me)
        def _():
            back[my_head] = res[run]

    for source in range(n):
        @pl.when(source != me)
        def _():
            arrived(ent.at[source], e_recv.at[source])
    ent_ref[...] = ent[...]
    for head in range(heads):
        @pl.when(head * group + owner_slot != me)
        def _():
            arrived(back.at[head], r_recv.at[head])
        out_ref[:, head * width:(head + 1) * width] = back[head]

    for step in range(1, n):
        peer = lax.rem(me + step, n)
        cols = columns(peer // group)
        sent(st_ref.at[peer], s_send.at[peer])
        sent(ebuf.at[peer], e_send.at[peer])
        sent(k_ref.at[:, cols], k_send.at[peer])
        sent(v_ref.at[:, cols], v_send.at[peer])
    for head in range(heads):
        @pl.when(head * group + owner_slot != me)
        def _():
            sent(q_ref.at[:, head * width:(head + 1) * width], q_send.at[head])

        @pl.when(head * group + flip(head, my_slot) != me)
        def _():
            sent(res.at[head], r_send.at[head])


def mix(n, heads, offsets, query, key, value, state, first_state, decay):
    rows = query.shape[0]
    width = query.shape[1] // heads
    vmem = pl.BlockSpec(memory_space=pltpu.VMEM)
    half = jnp.bfloat16
    slab = state.shape[1:]
    return pl.pallas_call(
        functools.partial(mixer_kernel, n, heads),
        out_shape=(
            jax.ShapeDtypeStruct(query.shape, half),
            jax.ShapeDtypeStruct(state.shape, half),
        ),
        in_specs=[pl.BlockSpec(memory_space=pltpu.SMEM)] + [vmem] * 6,
        out_specs=(vmem, vmem),
        scratch_shapes=[
            pltpu.VMEM((n, rows, width), half),
            pltpu.VMEM((n, rows, width), half),
            pltpu.VMEM((heads, rows, width), half),
            pltpu.VMEM((heads, rows, width), half),
            pltpu.VMEM((heads, rows, width), half),
            pltpu.VMEM((n,) + slab, half),
            pltpu.VMEM((n,) + slab, half),
            pltpu.VMEM((n,) + slab, half),
            *(pltpu.SemaphoreType.DMA((size,)) for size in (n, n, heads, heads, n, n) * 2),
        ],
        compiler_params=pltpu.CompilerParams(
            collective_id=0, has_side_effects=True, vmem_limit_bytes=40 * 2**20
        ),
        cost_estimate=pl.CostEstimate(
            flops=4 * 10**9, bytes_accessed=8 * 10**6, transcendentals=6 * 10**6
        ),
    )(offsets, query, key, value, state, first_state, decay)


def rotate(values, positions):
    half_width = values.shape[-1] // 2
    inverse = rope_base ** (-jnp.arange(half_width, dtype=jnp.float32) / half_width)
    angles = positions.astype(jnp.float32)[:, None] * inverse[None, :]
    cosine = jnp.cos(angles)[:, None, :]
    sine_table = jnp.sin(angles)[:, None, :]
    first_half = values[..., :half_width]
    second_half = values[..., half_width:]
    return jnp.concatenate(
        [
            first_half * cosine - second_half * sine_table,
            second_half * cosine + first_half * sine_table,
        ],
        axis=-1,
    )


def body(
    inputs,
    input_gain,
    stick_query_w,
    stick_key_w,
    stick_value_w,
    ret_query_w,
    ret_key_w,
    ret_value_w,
    stick_offset,
    ret_log_decay,
    initial_state,
    stick_gain,
    ret_gain,
    stick_out_w,
    ret_out_w,
):
    tok_rows = inputs.shape[0]
    matrices = (stick_query_w, stick_key_w, stick_value_w, ret_query_w, ret_key_w, ret_value_w)
    packed = jnp.concatenate([inputs, jnp.broadcast_to(input_gain[None, :], (16, inputs.shape[1]))])
    gathered = lax.all_gather(packed, "tp", axis=1, tiled=True)
    wide = gathered[:tok_rows].astype(jnp.float32)
    squares = jnp.sum(jnp.square(wide), axis=1)
    scaled = (wide * gathered[tok_rows].astype(jnp.float32)[None, :]).astype(jnp.bfloat16)
    stick_out_w, ret_out_w, scaled = lax.optimization_barrier((stick_out_w, ret_out_w, scaled))
    projected = tuple(
        (jnp.dot(scaled, matrix, preferred_element_type=jnp.float32) for matrix in matrices)
    )
    row_scale = lax.rsqrt(squares / D + epsilon)
    stick_query, stick_key, stick_value, ret_query, ret_key, ret_value = tuple(
        ((running * row_scale[:, None]).astype(jnp.bfloat16) for running in projected)
    )
    head_count = stick_offset.shape[0]
    head_width = stick_query.shape[1] // head_count
    first_pos = lax.axis_index("sp") * tok_rows
    query_pos = first_pos + jnp.arange(tok_rows, dtype=jnp.int32)
    ret_heads = ret_log_decay.shape[0]
    ret_width = ret_query.shape[1] // ret_heads
    turned_query = rotate(
        ret_query.reshape(tok_rows, ret_heads, ret_width).astype(jnp.float32), query_pos
    )
    turned_key = rotate(
        ret_key.reshape(tok_rows, ret_heads, ret_width).astype(jnp.float32), query_pos
    ) * ret_width ** (-0.5)
    ret_values = ret_value.reshape(tok_rows, ret_heads, ret_width)
    local_pos = jnp.arange(tok_rows, dtype=jnp.float32)
    distance = local_pos[:, None] - local_pos[None, :]
    decay_mask = jnp.where(
        distance[None] >= 0.0,
        jnp.exp(ret_log_decay[:, None, None] * jnp.maximum(distance, 0.0)[None]),
        0.0,
    )
    half = jnp.bfloat16
    key_decay = jnp.exp(ret_log_decay[None, :] * (tok_rows - 1.0 - local_pos[:, None]))
    own_state = jnp.einsum(
        "shd,she->hde", (turned_key * key_decay[:, :, None]).astype(half), ret_values,
        preferred_element_type=jnp.float32,
    )
    count = lax.axis_size("sp")
    slab = ret_width // count
    block_decay = jnp.exp(ret_log_decay * tok_rows)
    state_parts = jnp.swapaxes(
        own_state.astype(half).reshape(ret_heads, count, slab, ret_width), 0, 1
    ).reshape(count, ret_heads * slab, ret_width)
    stick_out, entering_parts = mix(
        count, head_count, stick_offset, stick_query, stick_key, stick_value, state_parts,
        initial_state.reshape(ret_heads * slab, ret_width),
        jnp.broadcast_to(
            block_decay[:, None, None], (ret_heads, slab, ret_width)
        ).reshape(ret_heads * slab, ret_width),
    )
    entering = jnp.swapaxes(
        entering_parts.reshape(count, ret_heads, slab, ret_width), 0, 1
    ).reshape(ret_heads, ret_width, ret_width)
    turned_query, turned_key = turned_query.astype(half), turned_key.astype(half)
    scores = (
        jnp.einsum("thd,shd->hts", turned_query, turned_key, preferred_element_type=jnp.float32)
        * decay_mask
    ).astype(half)
    inner_part = jnp.einsum("hts,she->the", scores, ret_values, preferred_element_type=jnp.float32)
    query_decay = jnp.exp(ret_log_decay[None, :] * (local_pos[:, None] + 1.0))
    cross_part = (
        jnp.einsum("thd,hde->the", turned_query, entering, preferred_element_type=jnp.float32)
        * query_decay[:, :, None]
    )
    ret_total = inner_part + cross_part
    centered = ret_total - jnp.mean(ret_total, axis=2, keepdims=True)
    normed = centered * lax.rsqrt(jnp.mean(centered * centered, axis=2, keepdims=True) + epsilon)
    ret_normed = (normed.reshape(tok_rows, ret_heads * ret_width) * ret_gain).astype(jnp.bfloat16)
    stick_total = stick_out.astype(jnp.float32)
    stick_squares = lax.psum(jnp.sum(jnp.square(stick_total), axis=1), "tp")
    stick_scale = lax.rsqrt(stick_squares / (STICK_HEADS * STICK_DIM) + epsilon)
    stick_normed = (stick_total * stick_scale[:, None] * stick_gain).astype(jnp.bfloat16)
    stick_cols, ret_cols = (
        lax.all_gather(stick_out_w, "sp", axis=1, tiled=True),
        lax.all_gather(ret_out_w, "sp", axis=1, tiled=True),
    )
    stick_part = jnp.dot(stick_normed, stick_cols, preferred_element_type=jnp.float32)
    return lax.psum_scatter(
        (stick_part + jnp.dot(ret_normed, ret_cols, preferred_element_type=jnp.float32)).astype(
            jnp.bfloat16
        ),
        "tp",
        scatter_dimension=0,
        tiled=True,
    )


def solution(mesh):
    in_specs = (
        P("sp", "tp"),
        P("tp"),
        P(None, "tp"),
        P(None, "tp"),
        P(None, "tp"),
        P(None, "tp"),
        P(None, "tp"),
        P(None, "tp"),
        P("tp"),
        P("tp"),
        P("tp", "sp", None),
        P("tp"),
        P("tp"),
        P("tp", "sp"),
        P("tp", "sp"),
    )
    out_specs = P(("sp", "tp"), None)
    return jax.shard_map(body, mesh=mesh, in_specs=in_specs, out_specs=out_specs, check_vma=False)
```

time: 599 us -> 257 us (0.43)
  waiting for transfers between devices: 412 us -> 58.5 us
  Pallas kernels: 0 us -> 127 us
  other arithmetic: 66 us -> 10.3 us
  blocking collectives: 50.3 us -> 2.47 us
  matrix products: 39.7 us -> 31.3 us
    all_gather x5 -> x1, waiting for transfers between devices: 258 us -> 12 us  [body(): gathered = lax.all_gather(packed, 'tp', axis=1, tiled=True)]
    pallas_call x0 -> x1, Pallas kernels: none -> 127 us  [mix(): pl.pallas_call(functools.partial(mixer_kernel, n, heads), out_shape=(jax....]
    all_gather x1, waiting for transfers between devices: 86.2 us -> 0.02 us  [body(): lax.all_gather(ret_out_w, 'sp', axis=1, tiled=True)]
    unnamed x1 -> x0, blocking collectives: 43.1 us -> none
    select_n x15 -> x0, other arithmetic: 41.1 us -> none  [hop(): jnp.where(position < mine, new, old)]
    all_gather x1, waiting for transfers between devices: 58.9 us -> 39.7 us  [body(): lax.all_gather(stick_out_w, 'sp', axis=1, tiled=True)]
    another operation x3 -> x1, other arithmetic: 12.8 us -> 2.64 us
    dot_general x6 -> x3, matrix products: 15.6 us -> 6.48 us  [the longest x1 2.87 us: body(): jnp.einsum('hts,she->the', scores, ret_values, preferred_element_type=jnp...]
  transfers between devices with their start and end apart: 8 -> 4, of which waited for: 8 -> 3; matrix products, arithmetic and copies ran while one was open for 18% -> 17% of each run, Pallas kernels for 0% -> 50%
where the time goes in v1:
time: 257 us; the launch traced here: 256 us
  Pallas kernels  127 us (49%)
  waiting for transfers between devices  58.5 us (23%)
  matrix products  31.3 us (12%)
  local copies, waits for them, and re-layouts  13.3 us (5%)
  between operations  13.3 us (5%)
  other arithmetic  10.3 us (4%)
    pallas_call x1, Pallas kernels, mix(): pl.pallas_call(functools.partial(mixer_kernel, n, heads), out_shape=(jax....  127 us
    all_gather x1, waiting for transfers between devices, body(): lax.all_gather(stick_out_w, 'sp', axis=1, tiled=True)  39.7 us
    dot_general x6, matrix products, body(): jnp.dot(scaled, matrix, preferred_element_type=jnp.float32)  16 us
    all_gather x1, waiting for transfers between devices, body(): gathered = lax.all_gather(packed, 'tp', axis=1, tiled=True)  12 us
    reduce_scatter x1, waiting for transfers between devices, body(): lax.psum_scatter((stick_part + jnp.dot(ret_normed, ret_cols, preferred_el...  6.73 us
  transfers between devices with their start and end apart: 4, of which 3 were waited for; matrix products, arithmetic and copies ran while one was open for 17% of the time, Pallas kernels for 50%

profile of v1, /device:TPU:0, one launch (start us, length us, event | category | flops | bytes accessed | tf_op | source)
XLA Modules:
  0.0 256.1 jit_solution(16482666088933875499)
XLA Ops:
  6.5 0.8 broadcast_in_dim.16
  7.4 1.9 pad_maximum_fusion.1
  9.4 12.0 %all-gather.4.cloned.1.call-done = bf16[272,2048]{1,0:T(8,128)(2,1)} async-done(((bf16[272,1024]{1,0:T(8,128)(2,1)}), bf16[272,2048]{1,0:T(8,128)(2,1)}) %all-gather.4.cloned.1.call-update) | async-done | bytes 1114128 | tf_op jit(solution)/shard_map/all_gather | solution.py:267
  21.3 0.8 slice_convert_fusion
  22.1 1.6 fusion.2
  24.0 0.7 fusion.30
  24.7 0.8 fusion.29
  25.5 1.2 multiply_cosine_fusion
  26.8 4.4 %fusion.6 = f32[256,1024]{1,0:T(8,128)} fusion(bf16[256,2048]{1,0:T(8,128)(2,1)S(1)} %get-tuple-element.10, bf16[2048,1024]{1,0:T(8,128)(2,1)} %param.21, f32[256]{0:T(256)S(1)} %add_rsqrt_fusion.2), kind=kOutput, calls=%fused_computation.15 | convolution fusion | flops 1074528256 | bytes 6292480 | tf_op jit(solution)/shard_map/dot_general | solution.py:273
  31.2 1.7 reshape.204
  32.9 4.9 %fusion.9 = f32[256,1024]{1,0:T(8,128)} fusion(bf16[256,2048]{1,0:T(8,128)(2,1)} %copy-done.3, bf16[2048,1024]{1,0:T(8,128)(2,1)} %param.20, f32[256]{0:T(256)S(1)} %add_rsqrt_fusion.2), kind=kOutput, calls=%fused_computation.18 | convolution fusion | flops 1074528256 | bytes 6292480 | tf_op jit(solution)/shard_map/dot_general | solution.py:273
  37.8 2.7 %reshape.205 = f32[256,4,256]{2,1,0:T(4,128)} reshape(f32[256,1024]{1,0:T(8,128)} %fusion.9) | data formatting | bytes 2097152 | tf_op jit(solution)/shard_map/convert_element_type | solution.py:286
  40.5 4.6 %fusion.7 = bf16[256,1024]{1,0:T(8,128)(2,1)} fusion(bf16[256,2048]{1,0:T(8,128)(2,1)} %copy-done.3, bf16[2048,1024]{1,0:T(8,128)(2,1)} %param.22, f32[256]{0:T(256)S(1)} %add_rsqrt_fusion.2), kind=kOutput, calls=%fused_computation.16 | convolution fusion | flops 1074266112 | bytes 5768192 | tf_op jit(solution)/shard_map/dot_general | solution.py:273
  45.0 2.0 copy.41
  47.1 2.7 %fusion.42 = (f32[256,4,128]{2,1,0:T(4,128)}, f32[256,4,128]{2,1,0:T(4,128)}, f32[256,4,128]{2,1,0:T(4,128)}, f32[256,4,128]{2,1,0:T(4,128)}) fusion(f32[256,4,256]{2,1,0:T(4,128)} %reshape.205, f32[256,4,256]{2,1,0:T(4,128)S(1)} %reshape.204), kind=kLoop, calls=%fused_computation.79 | loop fusion | bytes 4194304 | tf_op jit(solution)/shard_map/slice | solution.py:236
  49.8 2.6 %subtract_convert_fusion = (bf16[256,4,128]{2,0,1:T(8,128)(2,1)}, bf16[256,4,128]{2,0,1:T(8,128)(2,1)}, f32[256,4,128]{2,0,1:T(8,128)S(1)}, f32[256,4,128]{2,0,1:T(8,128)S(1)}) fusion(f32[256,4,128]{2,1,0:T(4,128)} %get-tuple-element.22, f32[256,4,128]{2,1,0:T(4,128)} %get-tuple-element.21, f32[256,128]{1,0:T(8,128)} %get-tuple-element.28, ...), kind=kLoop, calls=%fused_computation.49 | loop fusion | flops 1835008 | bytes 3932160 | tf_op jit(solution)/shard_map/convert.3
  52.4 1.7 convolution_convert_fusion
  54.2 0.7 fusion.11.q_ref
  55.0 0.8 copy-done.10
  55.8 0.7 fusion.12.k_ref
  56.5 0.9 copy-done.11
  57.4 0.7 fusion.13.v_ref
  58.3 126.9 %shard_map.145 = (bf16[256,512]{1,0:T(8,128)(2,1)S(1)}, bf16[16,64,256]{2,1,0:T(8,128)(2,1)S(1)}) custom-call(f32[4]{0:T(128)S(1)} %copy-done.2, bf16[256,512]{1,0:T(8,128)(2,1)S(1)} %fusion.11.q_ref, bf16[256,512]{1,0:T(8,128)(2,1)S(1)} %fusion.12.k_ref, bf16[256,512]{1,0:T(8,128)(2,1)S(1)} %fusion.13.v_ref, bf16[16,64,256]{2,1,0:T(8,128)(2,1)S(1)} %bitcast.41, ...), custom_call_target="tpu_custom_call" | custom-call | flops 4000000000 | bytes 8000000 | tf_op jit(solution)/shard_map/pallas_call | solution.py:202
  185.2 0.8 copy.33
  186.1 2.5 psum.7
  188.6 2.9 %convolution_bitcast_fusion.1 = f32[256,4,256]{0,2,1:T(8,128)} fusion(bf16[256,4,256]{0,2,1:T(8,128)(2,1)} %bitcast.45, f32[256,4,128]{2,0,1:T(8,128)S(1)} %get-tuple-element.25, f32[256,4,128]{2,0,1:T(8,128)S(1)} %get-tuple-element.26, f32[256,256]{1,0:T(8,128)} %fusion.29, f32[4]{0:T(128)S(1)} %copy-done.9, pred[256,256]{1,0:T(8,128)(4,1)S(1)} %copy-done.5, ...), kind=kOutput, calls=%fused_computation.9 | convolution fusion | flops 271319040 | bytes 3473424 | tf_op jit(solution)/shard_map/hts,she->the/dot_general | solution.py:326
  191.5 1.9 fusion.44
  193.7 0.4 copy-done.6
  194.3 4.8 %fusion.45 = f32[256,2048]{1,0:T(8,128)} fusion(bf16[256,1024]{0,1:T(8,128)(2,1)S(1)} %fusion.14, bf16[1024,2048]{1,0:T(8,128)(2,1)} %all-gather.8.cloned.1.call-done), kind=kOutput, calls=%fused_computation.82 | convolution fusion | flops 1073741824 | bytes 6815744 | tf_op jit(solution)/shard_map/dot_general | solution.py:346
  199.1 39.7 %all-gather.6.cloned.1.call-done = bf16[512,2048]{1,0:T(8,128)(2,1)} async-done(((bf16[512,128]{1,0:T(8,128)(2,1)}), bf16[512,2048]{1,0:T(8,128)(2,1)}) %all-gather.6.cloned.1.call-update) | async-done | bytes 2097168 | tf_op jit(solution)/shard_map/all_gather | solution.py:341
  238.9 4.0 %fusion = bf16[256,2048]{1,0:T(8,128)(2,1)} fusion(f32[256,2048]{1,0:T(8,128)} %fusion.45, bf16[512,2048]{1,0:T(8,128)(2,1)} %all-gather.6.cloned.1.call-done, bf16[256,512]{1,0:T(8,128)(2,1)S(1)} %get-tuple-element.11, f32[512]{0:T(512)S(1)} %copy-done.7, f32[256]{0:T(256)S(1)} %add_rsqrt_fusion.1), kind=kOutput, calls=%fused_computation.3 | convolution fusion | flops 538443776 | bytes 5508096 | tf_op jit(solution)/shard_map/dot_general | solution.py:344
  242.9 6.7 %reduce-scatter.2.cloned.1.call-done = bf16[128,2048]{1,0:T(8,128)(2,1)} async-done(((bf16[256,2048]{1,0:T(8,128)(2,1)}), bf16[128,2048]{1,0:T(8,128)(2,1)}) %reduce-scatter.2.cloned.1.call-update) | async-done | bytes 524304 | tf_op jit(solution)/shard_map/reduce_scatter | solution.py:345
  (47 shorter events, 1.3 us)
Async XLA Ops:
  6.5 47.7 %copy-start = (bf16[2048,512]{1,0:T(8,128)(2,1)S(1)}, bf16[2048,512]{1,0:T(8,128)(2,1)}, u32[]{:S(2)}) copy-start(bf16[2048,512]{1,0:T(8,128)(2,1)} %param.17) | copy-start | bytes 6291460
  6.5 17.3 %copy-start.8 = (f32[4]{0:T(128)S(1)}, f32[4]{0:T(128)}, u32[]{:S(2)}) copy-start(f32[4]{0:T(128)} %param.24) | copy-start | bytes 52
  6.5 14.8 %all-gather.4.cloned.1.call-start = ((), (), s32[]{:S(2)}) async-start(), calls=%async_computation.1 | async-start | bytes 1671168 | tf_op jit(solution)/shard_map/all_gather | solution.py:267
  9.3 185.0 %all-gather.8.cloned.1.call-start = ((), (), s32[]{:S(2)}) async-start(), calls=%async_computation.3 | async-start | bytes 4456448 | tf_op jit(solution)/shard_map/all_gather | solution.py:342
  23.7 3.0 %copy-start.3 = (bf16[256,2048]{1,0:T(8,128)(2,1)}, bf16[256,2048]{1,0:T(8,128)(2,1)S(1)}, u32[]{:S(2)}) copy-start(bf16[256,2048]{1,0:T(8,128)(2,1)S(1)} %get-tuple-element.10) | copy-start | bytes 3145732
  23.7 215.1 %all-gather.6.cloned.1.call-start = ((), (), s32[]{:S(2)}) async-start(), calls=%async_computation.2 | async-start | bytes 2228224 | tf_op jit(solution)/shard_map/all_gather | solution.py:341
  49.7 199.8 %reduce-scatter.2.cloned.1.call-start = ((), (), s32[]{:S(2)}) async-start(), calls=%async_computation.4 | async-start | bytes 1572864 | tf_op jit(solution)/shard_map/reduce_scatter | solution.py:345
  52.4 1.8 copy-start.4
  54.2 1.6 copy-start.10
  55.8 1.6 copy-start.11
  57.4 0.8 copy-start.1
  57.4 0.8 copy-start.2
  58.3 130.3 %copy-start.5 = (pred[256,256]{1,0:T(8,128)(4,1)S(1)}, pred[256,256]{1,0:T(8,128)(4,1)}, u32[]{:S(2)}) copy-start(pred[256,256]{1,0:T(8,128)(4,1)} %fusion.30) | copy-start | bytes 196612
  58.3 130.4 %copy-start.9 = (f32[4]{0:T(128)S(1)}, f32[4]{0:T(128)}, u32[]{:S(2)}) copy-start(f32[4]{0:T(128)} %param.24) | copy-start | bytes 52
  193.4 0.7 copy-start.6
  194.3 44.6 %copy-start.7 = (f32[512]{0:T(512)S(1)}, f32[512]{0:T(512)}, u32[]{:S(2)}) copy-start(f32[512]{0:T(512)} %param.26) | copy-start | bytes 6148
Sparse Core Ops, SparseCore 0:
  9.4 11.8 all-gather.3
  24.0 142.4 all-gather.7
  169.2 69.6 all-gather.5
  243.0 6.5 reduce-scatter.1
